TPU v7x, 256 devices: a 4x2x16 block of a 4x16x16 slice. The times are simulated.
256 devices in a mesh: grp: 2 (over y), fs: 16 (over z), tp: 8 (over x, core).
Axes of the slice: x: 4, y: 2, z: 16, core: 2. Of those that a mesh axis runs over, the one named last changes fastest.
The devices are a block of a 4x16x16 slice.
Arguments:
- tokens: bfloat16 [32768, 2048], P(('grp', 'fs', 'tp')), parts along dimension 0, may hold values from -12 to 12
- norm_gain: float32 [2048], replicated, may hold values from 0.1 to 1.9
- w_in: bfloat16 [2048, 8192], P('fs', 'tp'), may hold values from -0.125 to 0.125
- w_out: bfloat16 [8192, 2048], P('tp', 'fs'), may hold values from -0.0625 to 0.0625
Outputs:
- mixed: bfloat16 [32768, 2048], P(('grp', 'fs', 'tp')), parts along dimension 0
There are 2 independent parts, one for each index of `grp`. A program takes and returns all parts, laid end to end along the dimension named above; an argument that names none is the same for every part. Nothing has to cross between parts.
All inputs are finite; a program needn't handle non-finite values.
Results may differ from a plain program's by a relative error of at most 0.012.
Values may be sent and summed in bfloat16 or wider, within the bound.
A program may use at most 64 MiB of HBM per device.

v0:
```python
import jax
import jax.numpy as jnp
from jax import lax
from jax.sharding import PartitionSpec as P

EPS = 1e-06


def from_everyone(shard, axis):
    copies = jnp.broadcast_to(shard, (lax.axis_size(axis), *shard.shape))
    return lax.all_to_all(copies, axis, split_axis=0, concat_axis=0, tiled=True)


def joined_along(parts, dim):
    parts = jnp.moveaxis(parts, 0, dim)
    shape = parts.shape
    return parts.reshape(*shape[:dim], shape[dim] * shape[dim + 1], *shape[dim + 2 :])


def collect(shard, axis, dim):
    parts = from_everyone(shard, axis)
    return joined_along(parts, dim)


def local(tokens, norm_gain, w_in, w_out):
    xf = tokens.astype(jnp.float32)
    scale = lax.rsqrt(jnp.mean(xf * xf, axis=-1, keepdims=True) + EPS)
    normed = (xf * scale * norm_gain).astype(jnp.bfloat16)
    whole_in = lax.all_gather(w_in, "fs", axis=0, tiled=True)
    pre = jnp.dot(collect(normed, "tp", 0), whole_in, preferred_element_type=jnp.float32)
    hidden = jnp.square(jax.nn.relu(pre)).astype(jnp.bfloat16)
    whole_out = lax.all_gather(w_out, "fs", axis=1, tiled=True)
    summed = lax.psum_scatter(
        jnp.dot(hidden, whole_out, preferred_element_type=jnp.float32).astype(jnp.bfloat16),
        "tp",
        scatter_dimension=0,
        tiled=True,
    ).astype(jnp.float32)
    return (xf + summed).astype(jnp.bfloat16)


def solution(mesh):
    in_specs = (P(("grp", "fs", "tp"), None), P(), P("fs", "tp"), P("tp", "fs"))
    out_specs = P(("grp", "fs", "tp"), None)
    return jax.shard_map(local, mesh=mesh, in_specs=in_specs, out_specs=out_specs, check_vma=False)
```

profile of v0, /device:TPU:33, one launch (start us, length us, event | category | flops | bytes accessed | tf_op | source)
XLA Modules:
  0.0 252.1 jit_solution(16195759570042781914)
XLA Ops:
  6.5 0.0 all-gather.3.cloned.1.call-start
  6.6 0.7 all-gather.3.cloned.1.call-update
  7.3 0.1 all-gather.5.cloned.1.call-start
  7.4 0.7 all-gather.5.cloned.1.call-update
  8.1 0.1 reduce-scatter.2.cloned.1.call-start
  8.2 1.2 fusion
  9.4 1.2 fusion.2
  10.7 0.5 broadcast_in_dim.2
  11.2 72.4 %all_to_all.5 = bf16[8,128,2048]{2,1,0:T(8,128)(2,1)} all-to-all(bf16[8,128,2048]{2,1,0:T(8,128)(2,1)S(1)} %broadcast_in_dim.2), channel_id=1, replica_groups=mesh['grp'=2,'fs'=16,'tp'=8] {'tp'}, dimensions={0} | all-to-all | bytes 8388608 | tf_op jit(solution)/shard_map/all_to_all | solution.py:11
  83.6 8.1 %all-gather.3.cloned.1.call-done = bf16[2048,1024]{1,0:T(8,128)(2,1)} async-done(((bf16[128,1024]{1,0:T(8,128)(2,1)}), bf16[2048,1024]{1,0:T(8,128)(2,1)}) %all-gather.3.cloned.1.call-update) | async-done | bytes 4194320 | tf_op jit(solution)/shard_map/all_gather | solution.py:29
  91.7 90.1 %all-gather.5.cloned.1.call-done = bf16[1024,2048]{1,0:T(8,128)(2,1)} async-done(((bf16[1024,128]{1,0:T(8,128)(2,1)}), bf16[1024,2048]{1,0:T(8,128)(2,1)}) %all-gather.5.cloned.1.call-update) | async-done | bytes 4194320 | tf_op jit(solution)/shard_map/all_gather | solution.py:32
  181.8 14.4 %convolution_convert_fusion = bf16[1024,2048]{1,0:T(8,128)(2,1)} fusion(bf16[1024,2048]{1,0:T(8,128)(2,1)} %all-gather.5.cloned.1.call-done, bf16[1024,2048]{1,0:T(8,128)(2,1)} %bitcast.4, bf16[2048,1024]{1,0:T(8,128)(2,1)} %all-gather.3.cloned.1.call-done), kind=kOutput, calls=%fused_computation.1 | convolution fusion | flops 8595177472 | bytes 16777216 | tf_op jit(solution)/shard_map/dot_general | solution.py:34
  196.2 0.0 copy-start
  196.2 0.1 reduce-scatter.2.cloned.1.call-update
  196.2 47.4 %reduce-scatter.2.cloned.1.call-done = bf16[128,2048]{1,0:T(8,128)(2,1)} async-done(((bf16[1024,2048]{1,0:T(8,128)(2,1)}), bf16[128,2048]{1,0:T(8,128)(2,1)}) %reduce-scatter.2.cloned.1.call-update) | async-done | bytes 524304 | tf_op jit(solution)/shard_map/reduce_scatter | solution.py:33
  243.6 0.0 copy-done
  243.6 2.0 fusion.3
  (1 shorter events, 0.0 us)
Async XLA Ops:
  6.5 85.1 %all-gather.3.cloned.1.call-start = ((), (), s32[]{:S(2)}) async-start(), calls=%async_computation.2 | async-start | bytes 4456448 | tf_op jit(solution)/shard_map/all_gather | solution.py:29
  7.3 174.5 %all-gather.5.cloned.1.call-start = ((), (), s32[]{:S(2)}) async-start(), calls=%async_computation.3 | async-start | bytes 4456448 | tf_op jit(solution)/shard_map/all_gather | solution.py:32
  8.1 235.5 %reduce-scatter.2.cloned.1.call-start = ((), (), s32[]{:S(2)}) async-start(), calls=%async_computation.4 | async-start | bytes 4718592 | tf_op jit(solution)/shard_map/reduce_scatter | solution.py:33
  196.2 47.4 %copy-start = (bf16[128,2048]{1,0:T(8,128)(2,1)S(1)}, bf16[128,2048]{1,0:T(8,128)(2,1)}, u32[]{:S(2)}) copy-start(bf16[128,2048]{1,0:T(8,128)(2,1)} %param.4) | copy-start | bytes 1572868
Sparse Core Ops, SparseCore 0:
  9.1 82.4 all-gather.2
  93.4 88.3 all-gather.4
  196.4 47.2 reduce-scatter.1
where the time goes:
time: 253 us; the launch traced here: 252 us
  waiting for transfers between devices  147 us (58%)
  blocking collectives  72.4 us (29%)
  matrix products  14.4 us (6%)
  between operations  13.1 us (5%)
  other arithmetic  4.44 us (2%)
    all_gather x1, waiting for transfers between devices, local(): whole_out = lax.all_gather(w_out, 'fs', axis=1, tiled=True)  90.1 us
    all_to_all x1, blocking collectives, from_everyone(): return lax.all_to_all(copies, axis, split_axis=0, concat_axis=0, tiled=True)  72.4 us
    reduce_scatter x1, waiting for transfers between devices, local(): lax.psum_scatter(jnp.dot(hidden, whole_out, preferred_element_type=jnp.fl...  47.4 us
    dot_general x1, matrix products, local(): jnp.dot(hidden, whole_out, preferred_element_type=jnp.float32)  14.4 us
    all_gather x1, waiting for transfers between devices, local(): whole_in = lax.all_gather(w_in, 'fs', axis=0, tiled=True)  8.08 us
  transfers between devices with their start and end apart: 3, of which 3 were waited for; matrix products, arithmetic and copies ran while one was open for 1% of the time, Pallas kernels for 0%

commit v1 on v0

v1 whole, which is shorter than its diff:
```python
import functools

import jax
import jax.numpy as jnp
from jax import lax
from jax.experimental import pallas as pl
from jax.experimental.pallas import tpu as pltpu
from jax.sharding import PartitionSpec as P

EPS = 1e-06
F32, BF16 = jnp.float32, jnp.bfloat16
MESH = pl.DeviceIdType.MESH
IN_SHARED, OUT_SHARED = 3, 19


def kernel(n, tok_ref, gain_ref, win_ref, wout_ref, out_ref,
           normed, win_all, wout_all, acc, hidden,
           s1_send, s1_keep, d_recv, r1_send, l1_send, l1_recv, r1_recv, r2_send, l2_send, l2_recv, r2_recv,
           zs, zr, ys, yr, ts, tr, ds_, dr, s1s, s1r, xs, xr):
    half = n // 2
    g, z, t = lax.axis_index("grp"), lax.axis_index("fs"), lax.axis_index("tp")
    par = lax.rem(g, 2)
    partner = g + 1 - 2 * par
    x, c = t // 2, lax.rem(t, 2)
    oc = 1 - c
    xr_, xl_, xf_ = lax.rem(x + 1, 4), lax.rem(x + 3, 4), lax.rem(x + 2, 4)
    z_right, z_left = {"fs": lax.rem(z + 1, n)}, {"fs": lax.rem(z + n - 1, n)}
    x_right, x_left, sib = {"tp": 2 * xr_ + c}, {"tp": 2 * xl_ + c}, {"tp": 2 * x + oc}
    peer = {"grp": partner}
    tb, d = tok_ref.shape
    hb = tb // 2
    kb, ff = win_ref.shape
    cb = wout_ref.shape[1]
    started = []

    def remote(src, dst, send, recv, dev):
        return pltpu.make_async_remote_copy(
            src_ref=src, dst_ref=dst, send_sem=send, recv_sem=recv, device_id=dev, device_id_type=MESH)

    def go(copy):
        copy.start()
        started.append(copy)

    barrier = pltpu.get_barrier_semaphore()
    for dev in (z_right, z_left, x_right, x_left, sib, peer):
        pl.semaphore_signal(barrier, inc=1, device_id=dev, device_id_type=MESH)
    pl.semaphore_wait(barrier, 6)

    hops = ((half, half - 1), (half - 1, half))
    own, alls = (win_ref, wout_ref), (win_all, wout_all)
    b_in, b_out = IN_SHARED * 128, OUT_SHARED * 16
    a_in, a_out = ff - 2 * b_in, ff - 2 * b_out

    def slot(direction, k):
        return lax.rem(z - k + n, n) if direction == 0 else lax.rem(z + k, n)

    def region(w, piece, who):
        a, b, unit = ((a_in, b_in, 128), (a_out, b_out, 16))[w]
        part = pl.ds(0, a) if piece == 0 else pl.ds(pl.multiple_of(a + who * b, unit), b)
        return (slice(None), part) if w == 0 else (part, slice(None))

    def hop(w, direction, k, piece):
        s = slot(direction, k - 1)
        r = region(w, piece, par)
        dst = alls[w].at[(s, *r)]
        src = own[w].at[r] if k == 1 else dst
        return remote(src, dst, zs.at[w, direction, k - 1, piece], zr.at[w, direction, k - 1, piece],
                      (z_right, z_left)[direction])

    def hop_recv(w, direction, k, piece):
        ref = alls[w].at[(slot(direction, k), *region(w, piece, par))]
        remote(ref, ref, zs.at[w, direction, k - 1, piece], zr.at[w, direction, k - 1, piece],
               (z_right, z_left)[direction]).wait_recv()

    def share(w, direction, k, who):
        ref = alls[w].at[(slot(direction, k), *region(w, 1, who))]
        return remote(ref, ref, ys.at[w, direction, k - 1], yr.at[w, direction, k - 1], peer)

    def ring_own(w):
        for piece in (1, 0):
            for direction in (0, 1):
                go(hop(w, direction, 1, piece))

    def ring_slot(w, k):
        for piece in (1, 0):
            for direction in (0, 1):
                if k > hops[w][direction]:
                    continue
                hop_recv(w, direction, k, piece)
                if k < hops[w][direction]:
                    go(hop(w, direction, k + 1, piece))
                if piece == 1:
                    go(share(w, direction, k, par))

    def share_wait(w, k):
        for direction in (0, 1):
            if k <= hops[w][direction]:
                share(w, direction, k, 1 - par).wait_recv()

    ring_own(0)

    xf = tok_ref[...].astype(F32)
    scale = lax.rsqrt(jnp.mean(xf * xf, axis=-1, keepdims=True) + EPS)
    normed[c, x] = (xf * scale * gain_ref[...]).astype(BF16)
    acc[...] = jnp.zeros_like(acc)

    def rows(core, chip, h):
        return normed.at[core, chip, pl.ds(h * hb, hb)]

    def tok_send(direction, step):
        chip = x if step < 2 else (xl_, xr_)[direction]
        h = (0, 1, 0)[step] if direction == 0 else (1, 0, 1)[step]
        ref = rows(c, chip, h)
        return remote(ref, ref, ts.at[direction, step], tr.at[direction, step], (x_right, x_left)[direction])

    def tok_ref_in(core, direction, step):
        chip = ((xl_, xr_)[direction], (xl_, xr_)[direction], xf_)[step]
        h = (0, 1, 0)[step] if direction == 0 else (1, 0, 1)[step]
        return rows(core, chip, h)

    def tok_recv(direction, step):
        ref = tok_ref_in(c, direction, step)
        remote(ref, ref, ts.at[direction, step], tr.at[direction, step], (x_right, x_left)[direction]).wait_recv()

    def sib_copy(core, direction, step):
        ref = tok_ref_in(core, direction, step)
        return remote(ref, ref, ds_.at[direction, step], dr.at[direction, step], sib)

    def sib_own(core):
        ref = normed.at[core, x]
        return remote(ref, ref, ds_.at[0, 3], dr.at[0, 3], sib)

    for step in (0, 1):
        for direction in (0, 1):
            go(tok_send(direction, step))
    go(sib_own(c))

    def tok_slot(step):
        for direction in (0, 1):
            tok_recv(direction, step)
            if step == 0:
                go(tok_send(direction, 2))
            go(sib_copy(c, direction, step))

    def tok_wait(step):
        for direction in (0, 1):
            sib_copy(oc, direction, step).wait_recv()

    def product(chip, sa, sb, ra, rb):
        ca = pl.ds(pl.multiple_of(sa * kb, kb), kb)
        cb_ = pl.ds(pl.multiple_of(sb * kb, kb), kb)
        lhs = jnp.concatenate([normed[:, chip, :, ca], normed[:, chip, :, cb_]], axis=-1)
        rhs = jnp.concatenate([ra, rb], axis=0)
        return jnp.dot(lhs.reshape(2 * tb, 2 * kb), rhs, preferred_element_type=F32).reshape(2, tb, ff)

    def pre_add(chips, lo, hi):
        def step(j, _):
            sa, sb = lax.rem(z - j + n, n), lax.rem(z + j, n)
            for chip in chips:
                acc[:, chip] += product(chip, sa, sb, win_all[sa], win_all[sb])
            return 0
        if hi > lo:
            lax.fori_loop(lo, hi, step, 0)

    def finish_hidden():
        far = lax.rem(z + half, n)

        def step(chip, _):
            pre = acc[:, chip] + product(chip, z, far, win_ref[...], win_all[far])
            hidden[:, chip] = jnp.square(jnp.maximum(pre, 0.0)).astype(BF16)
            return 0
        lax.fori_loop(0, 4, step, 0)

    def width(q):
        return cb if q in (0, half) else 2 * cb

    def w_slice(q):
        return pl.ds(0, width(q))

    def s1(q):
        if q == 0:
            rhs = wout_ref[...]
        elif q == half:
            rhs = wout_all[lax.rem(z + half, n)]
        else:
            rhs = jnp.concatenate([wout_all[lax.rem(z - q + n, n)], wout_all[lax.rem(z + q, n)]], axis=1)
        wq = width(q)
        away = jnp.dot(hidden[oc].reshape(4 * tb, ff), rhs, preferred_element_type=F32)
        s1_send[q, :, :, :wq] = away.astype(BF16).reshape(4, tb, wq)
        kept = jnp.dot(hidden[c].reshape(4 * tb, ff), rhs, preferred_element_type=F32)
        s1_keep[q, :, :, :wq] = kept.reshape(4, tb, wq)

    def s1_copy(q):
        return remote(s1_send.at[q, :, :, w_slice(q)], d_recv.at[q, :, :, w_slice(q)], s1s.at[q], s1r.at[q], sib)

    def chip_sum(q, chip, h):
        part = pl.ds(h * hb, hb)
        wq = width(q)
        return s1_keep[q, chip, part, :wq] + d_recv[q, chip, part, :wq].astype(F32)

    def x_copy(q, kind):
        src, dst, dev = ((r1_send, l1_recv, x_right), (l1_send, r1_recv, x_left),
                         (r2_send, l2_recv, x_right), (l2_send, r2_recv, x_left))[kind]
        if kind < 2:
            src, dst = src.at[q, :, :, w_slice(q)], dst.at[q, :, :, w_slice(q)]
        else:
            src, dst = src.at[q, :, w_slice(q)], dst.at[q, :, w_slice(q)]
        return remote(src, dst, xs.at[kind, q], xr.at[kind, q], dev)

    def s2(q):
        s1_copy(q).wait_recv()
        wq = width(q)
        r1_send[q, 0, :, :wq] = chip_sum(q, xf_, 0).astype(BF16)
        r1_send[q, 1, :, :wq] = chip_sum(q, xr_, 1).astype(BF16)
        l1_send[q, 0, :, :wq] = chip_sum(q, xf_, 1).astype(BF16)
        l1_send[q, 1, :, :wq] = chip_sum(q, xl_, 0).astype(BF16)

    def s3(q):
        wq = width(q)
        x_copy(q, 0).wait_recv()
        r2_send[q, :, :wq] = (chip_sum(q, xr_, 0) + l1_recv[q, 0, :, :wq].astype(F32)).astype(BF16)
        x_copy(q, 1).wait_recv()
        l2_send[q, :, :wq] = (chip_sum(q, xl_, 1) + r1_recv[q, 0, :, :wq].astype(F32)).astype(BF16)

    def s4(q):
        wq = width(q)
        x_copy(q, 2).wait_recv()
        x_copy(q, 3).wait_recv()
        top = chip_sum(q, x, 0) + l2_recv[q, :, :wq].astype(F32) + r1_recv[q, 1, :, :wq].astype(F32)
        low = chip_sum(q, x, 1) + l1_recv[q, 1, :, :wq].astype(F32) + r2_recv[q, :, :wq].astype(F32)
        blocks = (z,) if q == 0 else (lax.rem(z + half, n),) if q == half else (lax.rem(z - q + n, n), lax.rem(z + q, n))
        for i, s in enumerate(blocks):
            cols = pl.ds(pl.multiple_of(s * cb, cb), cb)
            for h, part in ((0, top), (1, low)):
                rws = slice(h * hb, (h + 1) * hb)
                val = tok_ref[rws, cols].astype(F32) + part[:, i * cb:(i + 1) * cb]
                out_ref[rws, cols] = val.astype(BF16)

    def out_slot(s):
        if 0 <= s - 2 <= half:
            s2(s - 2)
        if 0 <= s - 3 <= half:
            s3(s - 3)
        if 0 <= s - 2 <= half:
            go(x_copy(s - 2, 0))
            go(x_copy(s - 2, 1))
        if 0 <= s - 4 <= half:
            s4(s - 4)
        if 0 <= s - 3 <= half:
            go(x_copy(s - 3, 2))
            go(x_copy(s - 3, 3))
        if 0 <= s - 1 <= half:
            if s > 1:
                share_wait(1, s - 1)
            s1(s - 1)
            go(s1_copy(s - 1))

    here, near, far = (x,), (xl_, xr_), (xf_,)
    when = {0: max(1, half * 3 // 8), 1: max(2, half * 4 // 8), 2: max(3, half * 6 // 8)}
    near_at, far_at = half * 6 // 8, half
    for k in range(1, half + 1):
        ring_slot(0, k)
        if k == half:
            ring_own(1)
        for step in (0, 1, 2):
            if when[step] == k:
                tok_slot(step)
        if k > 1:
            share_wait(0, k - 1)
        if k == 2:
            sib_own(oc).wait_recv()
        if k >= 2:
            pre_add(here, 1 if k == 2 else k - 1, k)
        if k == near_at:
            tok_wait(0)
            tok_wait(1)
        if k >= near_at:
            pre_add(near, 1 if k == near_at else k - 1, k)
        if k == far_at:
            tok_wait(2)
            pre_add(far, 1, k)
    for k in range(1, half + 1):
        ring_slot(1, k)
        if k == 1:
            share_wait(0, half)
            finish_hidden()
        out_slot(k)
    for s in range(half + 1, half + 5):
        out_slot(s)
    for copy in started:
        copy.wait_send()


def local(n, tokens, norm_gain, w_in, w_out):
    tb, d = tokens.shape
    kb, ff = w_in.shape
    cb = w_out.shape[1]
    half = n // 2
    q = half + 1
    dma = pltpu.SemaphoreType.DMA
    return pl.pallas_call(
        functools.partial(kernel, n),
        out_shape=jax.ShapeDtypeStruct((tb, d), BF16),
        in_specs=[pl.BlockSpec(memory_space=pltpu.VMEM)] * 4,
        out_specs=pl.BlockSpec(memory_space=pltpu.VMEM),
        scratch_shapes=[
            pltpu.VMEM((2, 4, tb, d), BF16),
            pltpu.VMEM((n, kb, ff), BF16),
            pltpu.VMEM((n, ff, cb), BF16),
            pltpu.VMEM((2, 4, tb, ff), F32),
            pltpu.VMEM((2, 4, tb, ff), BF16),
            pltpu.VMEM((q, 4, tb, 2 * cb), BF16),
            pltpu.VMEM((q, 4, tb, 2 * cb), F32),
            pltpu.VMEM((q, 4, tb, 2 * cb), BF16),
            pltpu.VMEM((q, 2, tb // 2, 2 * cb), BF16),
            pltpu.VMEM((q, 2, tb // 2, 2 * cb), BF16),
            pltpu.VMEM((q, 2, tb // 2, 2 * cb), BF16),
            pltpu.VMEM((q, 2, tb // 2, 2 * cb), BF16),
            pltpu.VMEM((q, tb // 2, 2 * cb), BF16),
            pltpu.VMEM((q, tb // 2, 2 * cb), BF16),
            pltpu.VMEM((q, tb // 2, 2 * cb), BF16),
            pltpu.VMEM((q, tb // 2, 2 * cb), BF16),
            dma((2, 2, half, 2)), dma((2, 2, half, 2)),
            dma((2, 2, half)), dma((2, 2, half)),
            dma((2, 3)), dma((2, 3)),
            dma((2, 4)), dma((2, 4)),
            dma((q,)), dma((q,)),
            dma((4, q)), dma((4, q)),
        ],
        compiler_params=pltpu.CompilerParams(collective_id=0, has_side_effects=True),
    )(tokens, norm_gain.reshape(1, d), w_in, w_out)


def solution(mesh):
    in_specs = (P(("grp", "fs", "tp"), None), P(), P("fs", "tp"), P("tp", "fs"))
    out_specs = P(("grp", "fs", "tp"), None)
    return jax.shard_map(functools.partial(local, mesh.shape["fs"]), mesh=mesh, in_specs=in_specs,
                         out_specs=out_specs, check_vma=False)
```

time: 253 us -> 120 us (0.47)
  waiting for transfers between devices: 147 us -> 0 us
  Pallas kernels: 0 us -> 116 us
  blocking collectives: 72.4 us -> 0 us
  matrix products: 14.4 us -> 0 us
  between operations: 13.1 us -> 0.01 us
  other arithmetic: 4.44 us -> 0 us
    pallas_call x0 -> x1, Pallas kernels: none -> 116 us  [local(): pl.pallas_call(functools.partial(kernel, n), out_shape=jax.ShapeDtypeStru...]
    all_gather x2 -> x0, waiting for transfers between devices: 98.2 us -> none  [the longest x1 90.1 us: local(): whole_out = lax.all_gather(w_out, 'fs', axis=1, tiled=True)]
    all_to_all x1 -> x0, blocking collectives: 72.4 us -> none  [from_everyone(): return lax.all_to_all(copies, axis, split_axis=0, concat_axis=0, tiled=True)]
    reduce_scatter x1 -> x0, waiting for transfers between devices: 47.4 us -> none  [local(): lax.psum_scatter(jnp.dot(hidden, whole_out, preferred_element_type=jnp.fl...]
    dot_general x1 -> x0, matrix products: 14.4 us -> none  [local(): jnp.dot(hidden, whole_out, preferred_element_type=jnp.float32)]
    convert_element_type x2 -> x0, other arithmetic: 3.2 us -> none  [the longest x1 1.96 us: local(): return (xf + summed).astype(jnp.bfloat16)]
  transfers between devices with their start and end apart: 3 -> 0, of which waited for: 3 -> 0; matrix products, arithmetic and copies ran while one was open for 1% -> 0% of each run, Pallas kernels for 0% -> 0%
where the time goes in v1:
time: 120 us; the launch traced here: 118 us
  Pallas kernels  116 us (97%)
  local copies, waits for them, and re-layouts  1.88 us (2%)
    pallas_call x1, Pallas kernels, local(): pl.pallas_call(functools.partial(kernel, n), out_shape=jax.ShapeDtypeStru...  116 us

profile of v1, /device:TPU:33, one launch (start us, length us, event | category | flops | bytes accessed | tf_op | source)
XLA Modules:
  0.0 118.3 jit_solution(14166210525395416579)
XLA Ops:
  0.0 116.4 %shard_map.46 = bf16[128,2048]{1,0:T(8,128)(2,1)} custom-call(bf16[128,2048]{1,0:T(8,128)(2,1)} %tok_ref.1, f32[1,2048]{1,0:T(1,128)} %bitcast.1, bf16[128,1024]{1,0:T(8,128)(2,1)} %win_ref.1, bf16[1024,128]{1,0:T(8,128)(2,1)} %wout_ref.1), custom_call_target="tpu_custom_call" | custom-call | tf_op jit(solution)/shard_map/pallas_call | solution.py:301
  116.4 1.9 %copy.6 = bf16[128,2048]{1,0:T(8,128)(2,1)} copy(bf16[128,2048]{1,0:T(8,128)(2,1)} %shard_map.46) | data formatting | bytes 1048576
